TPU v7x, 32 devices: a whole 2x2x4 slice. The times are simulated.
32 devices in a mesh: ra: 8 (over z, y), cb: 4 (over x, core).
Axes of the slice: x: 2, y: 2, z: 4, core: 2. Of those that a mesh axis runs over, the one named last changes fastest.
Arguments:
- tokens: bfloat16 [256, 3072], P(None, 'ra'), may hold values from -8 to 8, as said below
- first_gain: float32 [3072], P('ra'), may hold values from 0.1 to 1.9
- first_gate: float32 [3072, 8192], P('ra', 'cb'), may hold values from -0.109375 to 0.109375
- first_up: float32 [3072, 8192], P('ra', 'cb'), may hold values from -0.109375 to 0.109375
- first_down: float32 [8192, 3072], P('cb', 'ra'), may hold values from -0.0625 to 0.0625
- first_gate_scale: float32 [8192], P('cb'), may hold values from 0.5 to 2
- first_up_scale: float32 [8192], P('cb'), may hold values from 0.5 to 2
- first_down_scale: float32 [3072], P('ra'), may hold values from 0.5 to 2
- second_gain: float32 [3072], P('ra'), may hold values from 0.1 to 1.9
- second_gate: float32 [3072, 8192], P('ra', 'cb'), may hold values from -0.109375 to 0.109375
- second_up: float32 [3072, 8192], P('ra', 'cb'), may hold values from -0.109375 to 0.109375
- second_down: float32 [8192, 3072], P('cb', 'ra'), may hold values from -0.0625 to 0.0625
- second_gate_scale: float32 [8192], P('cb'), may hold values from 0.5 to 2
- second_up_scale: float32 [8192], P('cb'), may hold values from 0.5 to 2
- second_down_scale: float32 [3072], P('ra'), may hold values from 0.5 to 2
Outputs:
- mixed: bfloat16 [256, 3072], P(None, 'ra')
Inputs may be any that keep to these rules, and one draw needn't show every extreme that they name: The features come in groups of 64 with different magnitudes, and tokens differ in magnitude.
All inputs are finite; a program needn't handle non-finite values.
Results may differ from a plain program's by a relative error of at most 0.0093.
Values may be sent and summed in bfloat16 or wider, within the bound.
A program may use at most 64 MiB of HBM per device.

v0:
```python
import jax
import jax.numpy as jnp
from jax import lax
from jax.sharding import PartitionSpec as P

D = 3072


def half_step(stream_in, gain, w_gate, w_up, w_down, gate_scale, up_scale, down_scale):
    stream = stream_in.astype(jnp.float32)
    squares = jnp.sum(stream * stream, axis=1)
    shaped = (stream * gain[None, :]).astype(jnp.bfloat16)
    gate_part = jnp.dot(shaped, w_gate.astype(jnp.bfloat16), preferred_element_type=jnp.float32)
    up_part = jnp.dot(shaped, w_up.astype(jnp.bfloat16), preferred_element_type=jnp.float32)
    squares, gate_sum, up_sum = lax.psum((squares, gate_part, up_part), "ra")
    inverse = lax.rsqrt(squares / D + 1e-06)[:, None]
    gate_full = inverse * gate_scale[None, :] * gate_sum
    up_full = inverse * up_scale[None, :] * up_sum
    hidden = (jax.nn.silu(gate_full) * up_full).astype(jnp.bfloat16)
    down_part = jnp.dot(hidden, w_down.astype(jnp.bfloat16), preferred_element_type=jnp.float32)
    down_sum = lax.psum(down_part, "cb")
    return (stream + 0.5 * down_scale[None, :] * down_sum).astype(jnp.bfloat16)


def body(
    tokens,
    first_gain,
    first_gate,
    first_up,
    first_down,
    first_gate_scale,
    first_up_scale,
    first_down_scale,
    second_gain,
    second_gate,
    second_up,
    second_down,
    second_gate_scale,
    second_up_scale,
    second_down_scale,
):
    middle = half_step(
        tokens,
        first_gain,
        first_gate,
        first_up,
        first_down,
        first_gate_scale,
        first_up_scale,
        first_down_scale,
    )
    return half_step(
        middle,
        second_gain,
        second_gate,
        second_up,
        second_down,
        second_gate_scale,
        second_up_scale,
        second_down_scale,
    )


def solution(mesh):
    return jax.shard_map(
        body,
        mesh=mesh,
        in_specs=(
            P(None, "ra"),
            P("ra"),
            P("ra", "cb"),
            P("ra", "cb"),
            P("cb", "ra"),
            P("cb"),
            P("cb"),
            P("ra"),
            P("ra"),
            P("ra", "cb"),
            P("ra", "cb"),
            P("cb", "ra"),
            P("cb"),
            P("cb"),
            P("ra"),
        ),
        out_specs=P(None, "ra"),
        check_vma=False,
    )
```

profile of v0, /device:TPU:0, one launch (start us, length us, event | category | flops | bytes accessed | tf_op | source)
XLA Modules:
  0.0 416.3 jit_solution(14474829780918791749)
XLA Ops:
  6.5 0.0 all-reduce.13.cloned.1.call-start
  6.5 4.2 %fusion.10 = f32[256,2048]{1,0:T(8,128)} fusion(f32[384,2048]{1,0:T(8,128)} %param.17, bf16[256,384]{1,0:T(8,128)(2,1)} %param.15, f32[384]{0:T(512)} %param.16), kind=kOutput, calls=%fused_computation.12 | convolution fusion | flops 403734528 | bytes 5441024 | tf_op jit(solution)/shard_map/dot_general | solution.py:13
  10.7 0.0 copy-done
  10.8 0.0 copy-done.4
  10.8 0.0 copy-done.1
  10.8 2.0 fusion.8
  12.8 0.0 all-reduce.13.cloned.1.call-update
  12.8 0.0 all-reduce.7.cloned.1.call-start
  12.9 0.1 fusion.12
  13.0 24.3 %psum.56 = f32[256]{0:T(256)S(1)} all-reduce(f32[256]{0:T(256)S(1)} %fusion.12), channel_id=1, replica_groups=mesh['ra'=8,'cb'=4] {'ra'}, use_global_device_ids=true, to_apply=%region_1.0 | all-reduce | flops 256 | bytes 2048 | tf_op jit(solution)/shard_map/psum | solution.py:15
  37.3 135.1 %all-reduce.13.cloned.1.call-done = (f32[256,2048]{1,0:T(8,128)}, f32[256,2048]{1,0:T(8,128)}) async-done(((f32[256,2048]{1,0:T(8,128)}, f32[256,2048]{1,0:T(8,128)}), (f32[256,2048]{1,0:T(8,128)}, f32[256,2048]{1,0:T(8,128)})) %all-reduce.13.cloned.1.call-update) | async-done | bytes 4194320 | tf_op jit(solution)/shard_map/psum | solution.py:15
  172.4 0.0 copy-done.10
  172.4 0.0 copy-start.5
  172.4 5.1 %fusion.6 = f32[256,384]{1,0:T(8,128)} fusion(f32[2048,384]{1,0:T(8,128)} %param.19, f32[256,2048]{1,0:T(8,128)} %get-tuple-element.7, f32[256,2048]{1,0:T(8,128)} %get-tuple-element.8, f32[2048]{0:T(1024)S(1)} %copy-done.9, f32[2048]{0:T(1024)S(1)} %copy-done.10, f32[256]{0:T(256)S(1)} %add_rsqrt_fusion.1), kind=kOutput, calls=%fused_computation.8 | convolution fusion | flops 408682496 | bytes 7750656 | tf_op jit(solution)/shard_map/dot_general | solution.py:20
  177.5 0.0 all-reduce.7.cloned.1.call-update
  177.6 0.0 all-reduce.11.cloned.1.call-start
  177.6 31.9 %all-reduce.7.cloned.1.call-done = f32[256,384]{1,0:T(8,128)} async-done(((f32[256,384]{1,0:T(8,128)}), f32[256,384]{1,0:T(8,128)}) %all-reduce.7.cloned.1.call-update) | async-done | bytes 393232 | tf_op jit(solution)/shard_map/psum | solution.py:21
  209.5 1.1 fusion.15
  210.7 0.0 copy-done.5
  210.7 0.0 copy-start.3
  210.7 2.0 fusion.2
  212.7 0.3 copy-done.3
  213.1 2.1 fusion.4
  215.2 0.0 all-reduce.11.cloned.1.call-update
  215.2 0.0 all-reduce.9.cloned.1.call-start
  215.2 22.8 %psum.60 = f32[256]{0:T(256)S(1)} all-reduce(f32[256]{0:T(256)S(1)} %get-tuple-element.9), channel_id=1, replica_groups=mesh['ra'=8,'cb'=4] {'ra'}, use_global_device_ids=true, to_apply=%region_6.7 | all-reduce | flops 256 | bytes 2048 | tf_op jit(solution)/shard_map/psum | solution.py:15
  238.0 133.9 %all-reduce.11.cloned.1.call-done = (f32[256,2048]{1,0:T(8,128)}, f32[256,2048]{1,0:T(8,128)}) async-done(((f32[256,2048]{1,0:T(8,128)}, f32[256,2048]{1,0:T(8,128)}), (f32[256,2048]{1,0:T(8,128)}, f32[256,2048]{1,0:T(8,128)})) %all-reduce.11.cloned.1.call-update) | async-done | bytes 4194320 | tf_op jit(solution)/shard_map/psum | solution.py:15
  372.0 0.0 copy-done.12
  372.0 4.1 fusion
  376.0 0.0 all-reduce.9.cloned.1.call-update
  376.1 31.9 %all-reduce.9.cloned.1.call-done = f32[256,384]{1,0:T(8,128)} async-done(((f32[256,384]{1,0:T(8,128)}), f32[256,384]{1,0:T(8,128)}) %all-reduce.9.cloned.1.call-update) | async-done | bytes 393232 | tf_op jit(solution)/shard_map/psum | solution.py:21
  408.0 1.7 fusion.17
  (21 shorter events, 0.1 us)
Async XLA Ops:
  6.5 4.2 %copy-start = (bf16[256,384]{1,0:T(8,128)(2,1)S(1)}, bf16[256,384]{1,0:T(8,128)(2,1)}, u32[]{:S(2)}) copy-start(bf16[256,384]{1,0:T(8,128)(2,1)} %param.15) | copy-start | bytes 589828
  6.5 4.2 %copy-start.4 = (f32[384]{0:T(512)S(1)}, f32[384]{0:T(512)}, u32[]{:S(2)}) copy-start(f32[384]{0:T(512)} %param.16) | copy-start | bytes 4612
  6.5 4.2 %copy-start.1 = (f32[384,2048]{1,0:T(8,128)S(1)}, f32[384,2048]{1,0:T(8,128)}, u32[]{:S(2)}) copy-start(f32[384,2048]{1,0:T(8,128)} %param.18) | copy-start | bytes 9437188
  6.5 165.9 %all-reduce.13.cloned.1.call-start = ((), (), s32[]{:S(2)}) async-start(), calls=%async_computation.3 | async-start | bytes 8388608 | tf_op jit(solution)/shard_map/psum | solution.py:15
  12.8 159.6 %copy-start.9 = (f32[2048]{0:T(1024)S(1)}, f32[2048]{0:T(1024)}, u32[]{:S(2)}) copy-start(f32[2048]{0:T(1024)} %param.21) | copy-start | bytes 24580
  12.8 159.6 %copy-start.10 = (f32[2048]{0:T(1024)S(1)}, f32[2048]{0:T(1024)}, u32[]{:S(2)}) copy-start(f32[2048]{0:T(1024)} %param.20) | copy-start | bytes 24580
  12.8 196.7 %all-reduce.7.cloned.1.call-start = ((), (), s32[]{:S(2)}) async-start(), calls=%async_computation | async-start | bytes 786432 | tf_op jit(solution)/shard_map/psum | solution.py:21
  172.4 5.2 %copy-start.6 = (f32[384]{0:T(512)S(1)}, f32[384]{0:T(512)}, u32[]{:S(2)}) copy-start(f32[384]{0:T(512)} %param.22) | copy-start | bytes 4612
  172.4 38.3 %copy-start.2 = (f32[384,2048]{1,0:T(8,128)S(1)}, f32[384,2048]{1,0:T(8,128)}, u32[]{:S(2)}) copy-start(f32[384,2048]{1,0:T(8,128)} %param.25) | copy-start | bytes 9437188
  172.4 38.3 %copy-start.5 = (f32[384]{0:T(512)S(1)}, f32[384]{0:T(512)}, u32[]{:S(2)}) copy-start(f32[384]{0:T(512)} %param.23) | copy-start | bytes 4612
  177.6 194.4 %all-reduce.11.cloned.1.call-start = ((), (), s32[]{:S(2)}) async-start(), calls=%async_computation.2 | async-start | bytes 8388608 | tf_op jit(solution)/shard_map/psum | solution.py:15
  210.7 2.4 copy-start.3
  215.2 156.8 %copy-start.8 = (f32[2048,384]{1,0:T(8,128)S(1)}, f32[2048,384]{1,0:T(8,128)}, u32[]{:S(2)}) copy-start(f32[2048,384]{1,0:T(8,128)} %param.26) | copy-start | bytes 9437188
  215.2 156.8 %copy-start.11 = (f32[2048]{0:T(1024)S(1)}, f32[2048]{0:T(1024)}, u32[]{:S(2)}) copy-start(f32[2048]{0:T(1024)} %param.28) | copy-start | bytes 24580
  215.2 156.8 %copy-start.12 = (f32[2048]{0:T(1024)S(1)}, f32[2048]{0:T(1024)}, u32[]{:S(2)}) copy-start(f32[2048]{0:T(1024)} %param.27) | copy-start | bytes 24580
  215.2 192.8 %all-reduce.9.cloned.1.call-start = ((), (), s32[]{:S(2)}) async-start(), calls=%async_computation.1 | async-start | bytes 786432 | tf_op jit(solution)/shard_map/psum | solution.py:21
  372.0 4.1 copy-start.7
Sparse Core Ops, SparseCore 0:
  13.0 159.4 all-reduce.12
  177.7 31.7 all-reduce.6
  215.3 156.5 all-reduce.10
  376.2 31.7 all-reduce.8
where the time goes:
time: 417 us; the launch traced here: 416 us
  waiting for transfers between devices  333 us (80%)
  blocking collectives  47 us (11%)
  matrix products  19.6 us (5%)
  between operations  13.2 us (3%)
    psum x2, waiting for transfers between devices, half_step(): squares, gate_sum, up_sum = lax.psum((squares, gate_part, up_part), 'ra')  269 us
    psum x2, waiting for transfers between devices, half_step(): down_sum = lax.psum(down_part, 'cb')  63.8 us
    psum x2, blocking collectives, half_step(): squares, gate_sum, up_sum = lax.psum((squares, gate_part, up_part), 'ra')  47 us
    dot_general x2, matrix products, half_step(): jnp.dot(hidden, w_down.astype(jnp.bfloat16), preferred_element_type=jnp.f...  9.19 us
  transfers between devices with their start and end apart: 4, of which 4 were waited for; matrix products, arithmetic and copies ran while one was open for 0% of the time, Pallas kernels for 0%

commit v1 on v0

--- a/solution.py
+++ b/solution.py
@@ -18,7 +18,7 @@
     up_full = inverse * up_scale[None, :] * up_sum
     hidden = (jax.nn.silu(gate_full) * up_full).astype(jnp.bfloat16)
     down_part = jnp.dot(hidden, w_down.astype(jnp.bfloat16), preferred_element_type=jnp.float32)
-    down_sum = lax.psum(down_part, "cb")
+    down_sum = jnp.sum(lax.all_gather(down_part, "cb"), axis=0)
     return (stream + 0.5 * down_scale[None, :] * down_sum).astype(jnp.bfloat16)
 
 

time: 417 us -> 392 us (0.940)
  waiting for transfers between devices: 333 us -> 306 us
    psum x2 -> x0, waiting for transfers between devices: 63.8 us -> none  [half_step(): down_sum = lax.psum(down_part, 'cb')]
    all_gather x0 -> x2, waiting for transfers between devices: none -> 37.5 us  [half_step(): down_sum = jnp.sum(lax.all_gather(down_part, 'cb'), axis=0)]
where the time goes in v1:
time: 392 us
  waiting for transfers between devices  306 us (78%)
  blocking collectives  47.1 us (12%)
  matrix products  18.5 us (5%)
  between operations  13.2 us (3%)
  other arithmetic  5.83 us (1%)
    psum x2, waiting for transfers between devices, half_step(): squares, gate_sum, up_sum = lax.psum((squares, gate_part, up_part), 'ra')  269 us
    psum x2, blocking collectives, half_step(): squares, gate_sum, up_sum = lax.psum((squares, gate_part, up_part), 'ra')  47.1 us
    all_gather x2, waiting for transfers between devices, half_step(): down_sum = jnp.sum(lax.all_gather(down_part, 'cb'), axis=0)  37.5 us
    dot_general x2, matrix products, half_step(): jnp.dot(hidden, w_down.astype(jnp.bfloat16), preferred_element_type=jnp.f...  8.08 us
  transfers between devices with their start and end apart: 4, of which 4 were waited for; matrix products, arithmetic and copies ran while one was open for 0% of the time, Pallas kernels for 0%

profile of v1, /device:TPU:0, one launch (start us, length us, event | category | flops | bytes accessed | tf_op | source)
XLA Modules:
  0.0 391.6 jit_solution(6429474965641833515)
XLA Ops:
  6.5 0.0 all-reduce.7.cloned.1.call-start
  6.5 4.2 %fusion.10 = f32[256,2048]{1,0:T(8,128)} fusion(f32[384,2048]{1,0:T(8,128)} %param.17, bf16[256,384]{1,0:T(8,128)(2,1)} %param.15, f32[384]{0:T(512)} %param.16), kind=kOutput, calls=%fused_computation.12 | convolution fusion | flops 403734528 | bytes 5441024 | tf_op jit(solution)/shard_map/dot_general | solution.py:13
  10.8 0.0 copy-done
  10.8 0.0 copy-done.4
  10.8 2.1 fusion.8
  12.8 0.0 all-reduce.7.cloned.1.call-update
  12.9 0.0 all-gather.5.cloned.1.call-start
  12.9 0.1 fusion.12
  13.0 24.3 %psum.42 = f32[256]{0:T(256)S(1)} all-reduce(f32[256]{0:T(256)S(1)} %fusion.12), channel_id=1, replica_groups=mesh['ra'=8,'cb'=4] {'ra'}, use_global_device_ids=true, to_apply=%region_1.0 | all-reduce | flops 256 | bytes 2048 | tf_op jit(solution)/shard_map/psum | solution.py:15
  37.4 135.0 %all-reduce.7.cloned.1.call-done = (f32[256,2048]{1,0:T(8,128)}, f32[256,2048]{1,0:T(8,128)}) async-done(((f32[256,2048]{1,0:T(8,128)}, f32[256,2048]{1,0:T(8,128)}), (f32[256,2048]{1,0:T(8,128)}, f32[256,2048]{1,0:T(8,128)})) %all-reduce.7.cloned.1.call-update) | async-done | bytes 4194320 | tf_op jit(solution)/shard_map/psum | solution.py:15
  172.4 0.0 copy-done.8
  172.4 4.0 %fusion.6 = f32[256,384]{1,0:T(8,128)} fusion(f32[2048,384]{1,0:T(8,128)S(1)} %copy-done.8, f32[256,2048]{1,0:T(8,128)} %get-tuple-element.7, f32[256,2048]{1,0:T(8,128)} %get-tuple-element.8, f32[2048]{0:T(1024)S(1)} %copy-done.10, f32[2048]{0:T(1024)S(1)} %copy-done.11, f32[256]{0:T(256)S(1)} %add_rsqrt_fusion.1), kind=kOutput, calls=%fused_computation.8 | convolution fusion | flops 408682496 | bytes 7750656 | tf_op jit(solution)/shard_map/dot_general | solution.py:20
  176.4 0.0 all-gather.5.cloned.1.call-update
  176.4 0.0 all-reduce.5.cloned.1.call-start
  176.5 18.7 %all-gather.5.cloned.1.call-done = f32[1024,384]{1,0:T(8,128)} async-done(((f32[256,384]{1,0:T(8,128)}), f32[1024,384]{1,0:T(8,128)}) %all-gather.5.cloned.1.call-update) | async-done | bytes 1572880 | tf_op jit(solution)/shard_map/all_gather | solution.py:21
  195.2 2.3 reduce_sum.37
  197.5 1.1 fusion.15
  198.7 0.0 copy-start.3
  198.7 2.0 fusion.2
  200.7 0.3 copy-done.3
  201.0 2.1 fusion.4
  203.1 0.0 all-reduce.5.cloned.1.call-update
  203.2 0.0 all-gather.7.cloned.1.call-start
  203.2 22.8 %psum.45 = f32[256]{0:T(256)S(1)} all-reduce(f32[256]{0:T(256)S(1)} %get-tuple-element.9), channel_id=1, replica_groups=mesh['ra'=8,'cb'=4] {'ra'}, use_global_device_ids=true, to_apply=%region_6.7 | all-reduce | flops 256 | bytes 2048 | tf_op jit(solution)/shard_map/psum | solution.py:15
  226.0 133.9 %all-reduce.5.cloned.1.call-done = (f32[256,2048]{1,0:T(8,128)}, f32[256,2048]{1,0:T(8,128)}) async-done(((f32[256,2048]{1,0:T(8,128)}, f32[256,2048]{1,0:T(8,128)}), (f32[256,2048]{1,0:T(8,128)}, f32[256,2048]{1,0:T(8,128)})) %all-reduce.5.cloned.1.call-update) | async-done | bytes 4194320 | tf_op jit(solution)/shard_map/psum | solution.py:15
  359.9 0.0 copy-done.9
  359.9 4.1 %fusion = f32[256,384]{1,0:T(8,128)} fusion(f32[2048,384]{1,0:T(8,128)S(1)} %copy-done.9, f32[256,2048]{1,0:T(8,128)} %get-tuple-element.5, f32[256,2048]{1,0:T(8,128)} %get-tuple-element.6, f32[2048]{0:T(1024)S(1)} %copy-done.12, f32[2048]{0:T(1024)S(1)} %copy-done.13, f32[256]{0:T(256)S(1)} %add_rsqrt_fusion), kind=kOutput, calls=%fused_computation.2 | convolution fusion | flops 408682496 | bytes 7750656 | tf_op jit(solution)/shard_map/dot_general | solution.py:20
  364.0 0.0 all-gather.7.cloned.1.call-update
  364.0 0.0 copy-done.7
  364.0 18.8 %all-gather.7.cloned.1.call-done = f32[1024,384]{1,0:T(8,128)} async-done(((f32[256,384]{1,0:T(8,128)}), f32[1024,384]{1,0:T(8,128)}) %all-gather.7.cloned.1.call-update) | async-done | bytes 1572880 | tf_op jit(solution)/shard_map/all_gather | solution.py:21
  382.8 1.5 reduce_sum.39
  384.3 0.7 fusion.17
  (25 shorter events, 0.1 us)
Async XLA Ops:
  6.5 4.2 %copy-start = (bf16[256,384]{1,0:T(8,128)(2,1)S(1)}, bf16[256,384]{1,0:T(8,128)(2,1)}, u32[]{:S(2)}) copy-start(bf16[256,384]{1,0:T(8,128)(2,1)} %param.15) | copy-start | bytes 589828
  6.5 4.2 %copy-start.4 = (f32[384]{0:T(512)S(1)}, f32[384]{0:T(512)}, u32[]{:S(2)}) copy-start(f32[384]{0:T(512)} %param.16) | copy-start | bytes 4612
  6.5 4.2 %copy-start.1 = (f32[384,2048]{1,0:T(8,128)S(1)}, f32[384,2048]{1,0:T(8,128)}, u32[]{:S(2)}) copy-start(f32[384,2048]{1,0:T(8,128)} %param.18) | copy-start | bytes 9437188
  6.5 165.8 %all-reduce.7.cloned.1.call-start = ((), (), s32[]{:S(2)}) async-start(), calls=%async_computation.3 | async-start | bytes 8388608 | tf_op jit(solution)/shard_map/psum | solution.py:15
  12.8 159.5 %copy-start.8 = (f32[2048,384]{1,0:T(8,128)S(1)}, f32[2048,384]{1,0:T(8,128)}, u32[]{:S(2)}) copy-start(f32[2048,384]{1,0:T(8,128)} %param.19) | copy-start | bytes 9437188
  12.8 159.5 %copy-start.10 = (f32[2048]{0:T(1024)S(1)}, f32[2048]{0:T(1024)}, u32[]{:S(2)}) copy-start(f32[2048]{0:T(1024)} %param.21) | copy-start | bytes 24580
  12.8 159.5 %copy-start.11 = (f32[2048]{0:T(1024)S(1)}, f32[2048]{0:T(1024)}, u32[]{:S(2)}) copy-start(f32[2048]{0:T(1024)} %param.20) | copy-start | bytes 24580
  12.9 182.3 %all-gather.5.cloned.1.call-start = ((), (), s32[]{:S(2)}) async-start(), calls=%async_computation | async-start | bytes 1966080 | tf_op jit(solution)/shard_map/all_gather | solution.py:21
  172.4 4.1 %copy-start.6 = (f32[384]{0:T(512)S(1)}, f32[384]{0:T(512)}, u32[]{:S(2)}) copy-start(f32[384]{0:T(512)} %param.22) | copy-start | bytes 4612
  176.4 22.3 %copy-start.2 = (f32[384,2048]{1,0:T(8,128)S(1)}, f32[384,2048]{1,0:T(8,128)}, u32[]{:S(2)}) copy-start(f32[384,2048]{1,0:T(8,128)} %param.25) | copy-start | bytes 9437188
  176.4 22.3 %copy-start.5 = (f32[384]{0:T(512)S(1)}, f32[384]{0:T(512)}, u32[]{:S(2)}) copy-start(f32[384]{0:T(512)} %param.23) | copy-start | bytes 4612
  176.4 183.5 %all-reduce.5.cloned.1.call-start = ((), (), s32[]{:S(2)}) async-start(), calls=%async_computation.2 | async-start | bytes 8388608 | tf_op jit(solution)/shard_map/psum | solution.py:15
  198.7 2.4 copy-start.3
  203.1 156.8 %copy-start.9 = (f32[2048,384]{1,0:T(8,128)S(1)}, f32[2048,384]{1,0:T(8,128)}, u32[]{:S(2)}) copy-start(f32[2048,384]{1,0:T(8,128)} %param.26) | copy-start | bytes 9437188
  203.1 156.8 %copy-start.12 = (f32[2048]{0:T(1024)S(1)}, f32[2048]{0:T(1024)}, u32[]{:S(2)}) copy-start(f32[2048]{0:T(1024)} %param.28) | copy-start | bytes 24580
  203.1 156.8 %copy-start.13 = (f32[2048]{0:T(1024)S(1)}, f32[2048]{0:T(1024)}, u32[]{:S(2)}) copy-start(f32[2048]{0:T(1024)} %param.27) | copy-start | bytes 24580
  203.2 179.7 %all-gather.7.cloned.1.call-start = ((), (), s32[]{:S(2)}) async-start(), calls=%async_computation.1 | async-start | bytes 1966080 | tf_op jit(solution)/shard_map/all_gather | solution.py:21
  359.9 4.1 %copy-start.7 = (f32[384]{0:T(512)S(1)}, f32[384]{0:T(512)}, u32[]{:S(2)}) copy-start(f32[384]{0:T(512)} %param.29) | copy-start | bytes 4612
Sparse Core Ops, SparseCore 0:
  13.0 159.3 all-reduce.6
  176.5 18.6 all-gather.4
  203.3 156.5 all-reduce.4
  364.1 18.6 all-gather.6
